TPU v7x, 32 devices: a whole 2x2x4 slice. The times are simulated.
32 devices in a mesh: sp: 8 (over z, x), tp: 4 (over y, core).
Axes of the slice: x: 2, y: 2, z: 4, core: 2. Of those that a mesh axis runs over, the one named last changes fastest.
Arguments:
- queries: bfloat16 [2048, 1024], P('sp', 'tp'), may hold values from -6 to 6
- keys: bfloat16 [2048, 256], P('sp'), may hold values from -6 to 6
- values: bfloat16 [2048, 256], P('sp'), may hold values from -6 to 6
- sink: float32 [16], P('tp'), may hold values from 3 to 6
- w_out: bfloat16 [1024, 2048], P('tp'), may hold values from -0.1875 to 0.1875
- stream: bfloat16 [2048, 2048], P(('sp', 'tp')), may hold values from -6 to 6
- gain: bfloat16 [2048], replicated, may hold values from 0.099609375 to 1.8984375
- routes: int32 [2048, 4], P('sp'), may hold values from 0 to 63, all different within a row; in each aligned block of 64 rows (0 to 63, 64 to 127, ...) at most 8 rows name the same one
- route_weights: float32 [2048, 4], P('sp'), may hold values from 0.2 to 1
- w_gate: bfloat16 [64, 1024, 2048], P('sp', 'tp'), may hold values from -0.125 to 0.125
- w_up: bfloat16 [64, 1024, 2048], P('sp', 'tp'), may hold values from -0.125 to 0.125
- w_down: bfloat16 [64, 1024, 2048], P('sp', None, 'tp'), may hold values from -0.1875 to 0.1875
- shared_gate: bfloat16 [1024, 2048], P('tp'), may hold values from -0.125 to 0.125
- shared_up: bfloat16 [1024, 2048], P('tp'), may hold values from -0.125 to 0.125
- shared_down: bfloat16 [1024, 2048], P(None, 'tp'), may hold values from -0.1875 to 0.1875
Outputs:
- layer_out: bfloat16 [2048, 2048], P('sp', 'tp')
Inputs may be any that keep to these rules, and one draw needn't show every extreme that they name: `routes`: in each aligned block of 64 rows no expert is named in more than 8 rows, and some blocks reach 8; a row names 4 different experts.
All inputs are finite; a program needn't handle non-finite values.
Results may differ from a plain program's by a relative error of at most 0.014.
Values may be sent and summed in bfloat16 or wider, within the bound.
A program may use at most 128 MiB of HBM per device.

v0:
```python
import jax
import jax.numpy as jnp
from jax import lax
from jax.sharding import PartitionSpec as P

D = 2048
HEADS = 16
KV_HEADS = 4
HD = 64
WINDOW = 128
EXPERTS = 64
TOPK = 4
NORM_EPS = 1e-05


def with_halo(array, sides, width):
    for axis, dim in sides:
        devices, length = (lax.axis_size(axis), array.shape[dim])
        up = [(i, (i + 1) % devices) for i in range(devices - 1)]
        down = [(j, i) for i, j in up]
        last = lax.slice_in_dim(array, length - width, length, axis=dim)
        leading = lax.slice_in_dim(array, 0, width, axis=dim)
        before = lax.ppermute(last, axis, up)
        after = lax.ppermute(leading, axis, down)
        array = jnp.concatenate([before, array, after], axis=dim)
    return array


def slot_ids(block_routes, capacity):
    flat_routes = block_routes.reshape(-1)
    hit_table = (flat_routes[:, None] == jnp.arange(EXPERTS)[None, :]).astype(jnp.int32)
    earlier = jnp.cumsum(hit_table, axis=0) - hit_table
    slot_rank = jnp.sum(earlier * hit_table, axis=1)
    return flat_routes * capacity + slot_rank


def local(
    queries,
    keys,
    values,
    sink,
    w_out,
    stream,
    gain,
    routes,
    route_weights,
    w_gate,
    w_up,
    w_down,
    shared_gate,
    shared_up,
    shared_down,
):
    tok_dev = queries.shape[0]
    n_tp = lax.axis_size("tp")
    n_sp = lax.axis_size("sp")
    tp_idx = lax.axis_index("tp")
    sp_idx = lax.axis_index("sp")
    heads_dev = HEADS // n_tp
    group = HEADS // KV_HEADS
    kv_head = tp_idx * heads_dev // group
    key_own = lax.dynamic_slice_in_dim(keys, kv_head * HD, HD, 1)
    value_own = lax.dynamic_slice_in_dim(values, kv_head * HD, HD, 1)
    paired = jnp.concatenate([key_own, value_own], axis=1)
    padded = with_halo(paired, (("sp", 0),), WINDOW)
    blocks = tok_dev // WINDOW
    framed = padded.reshape(blocks + 2, WINDOW, 2 * HD)
    banded = jnp.concatenate([framed[:-2], framed[1:-1], framed[2:]], axis=1)
    key_band = banded[:, :, :HD]
    value_band = banded[:, :, HD:]
    query_blocks = queries.reshape(blocks, WINDOW, heads_dev, HD)
    scores = jnp.einsum(
        "nqhd,njd->nhqj", query_blocks, key_band, preferred_element_type=jnp.float32
    ) * HD ** (-0.5)
    offset = sp_idx * tok_dev
    seq_total = tok_dev * n_sp
    query_pos = (
        offset + jnp.arange(blocks)[:, None, None] * WINDOW + jnp.arange(WINDOW)[None, :, None]
    )
    key_pos = (
        offset
        - WINDOW
        + jnp.arange(blocks)[:, None, None] * WINDOW
        + jnp.arange(3 * WINDOW)[None, None, :]
    )
    allowed = (jnp.abs(query_pos - key_pos) <= WINDOW) & (key_pos >= 0) & (key_pos < seq_total)
    scores = jnp.where(allowed[:, None], scores, -jnp.inf)
    sink_level = sink.reshape(1, heads_dev, 1, 1)
    row_peak = jnp.maximum(scores.max(-1, keepdims=True), sink_level)
    probabilities = jnp.exp(scores - row_peak)
    denominator = probabilities.sum(-1, keepdims=True) + jnp.exp(sink_level - row_peak)
    weights = (probabilities / denominator).astype(jnp.bfloat16)
    attended = jnp.einsum("nhqj,njd->nqhd", weights, value_band, preferred_element_type=jnp.float32)
    attended = attended.astype(jnp.bfloat16).reshape(tok_dev, heads_dev * HD)
    rows_dev = tok_dev // n_tp
    d_dev = w_down.shape[2]
    projected = lax.psum_scatter(
        jnp.dot(attended, w_out, preferred_element_type=jnp.float32),
        "tp",
        scatter_dimension=0,
        tiled=True,
    )
    mixed_rows = (stream.astype(jnp.float32) + projected).astype(jnp.bfloat16)
    whole_rows = lax.all_gather(mixed_rows, "tp", axis=0, tiled=True)
    wide_rows = whole_rows.astype(jnp.float32)
    scale_rows = lax.rsqrt(jnp.mean(wide_rows * wide_rows, axis=-1, keepdims=True) + NORM_EPS)
    normed = (wide_rows * scale_rows * gain.astype(jnp.float32)).astype(jnp.bfloat16)
    residual = lax.dynamic_slice_in_dim(wide_rows, tp_idx * d_dev, d_dev, 1)
    exp_dev = w_gate.shape[0]
    capacity = max(1, 2 * tok_dev * TOPK // (n_tp * EXPERTS))
    slot_count = EXPERTS * capacity
    blocked_routes = routes.reshape(n_tp, rows_dev, TOPK)
    destination = jax.vmap(lambda block_routes: slot_ids(block_routes, capacity))(blocked_routes)
    slot_select = destination[:, None, :] == jnp.arange(slot_count)[None, :, None]
    slot_select = slot_select.reshape(n_tp, slot_count, rows_dev, TOPK).astype(jnp.float32)
    dispatch_table = jnp.sum(slot_select, axis=-1).astype(jnp.bfloat16)
    combine_table = jnp.sum(slot_select * route_weights.reshape(n_tp, 1, rows_dev, TOPK), axis=-1)
    normed_blocks = normed.reshape(n_tp, rows_dev, D)
    own_table = lax.dynamic_index_in_dim(dispatch_table, tp_idx, 0, keepdims=False)
    own_rows = lax.dynamic_index_in_dim(normed_blocks, tp_idx, 0, keepdims=False)
    outgoing = jnp.dot(own_table, own_rows, preferred_element_type=jnp.float32).astype(jnp.bfloat16)
    arrived = lax.all_to_all(outgoing, "sp", split_axis=0, concat_axis=0, tiled=True)
    arrived = arrived.reshape(1, n_sp, exp_dev, capacity, D)
    piece_rows = lax.all_gather(arrived, "tp", axis=0, tiled=True)
    gate_act = jnp.einsum(
        "tsecd,efd->tsecf", piece_rows, w_gate, preferred_element_type=jnp.float32
    )
    up_act = jnp.einsum("tsecd,efd->tsecf", piece_rows, w_up, preferred_element_type=jnp.float32)
    hidden = (jax.nn.silu(gate_act) * up_act).astype(jnp.bfloat16)
    shared_gate_act = jnp.einsum(
        "td,fd->tf", normed, shared_gate, preferred_element_type=jnp.float32
    )
    shared_up_act = jnp.einsum("td,fd->tf", normed, shared_up, preferred_element_type=jnp.float32)
    shared_hidden = (jax.nn.silu(shared_gate_act) * shared_up_act).astype(jnp.bfloat16)
    shared_hidden = shared_hidden.reshape(1, 1, 1, tok_dev, shared_hidden.shape[1])
    expert_piece = lax.all_gather(hidden, "tp", axis=4, tiled=True)
    shared_piece = lax.all_gather(shared_hidden, "tp", axis=4, tiled=True)
    piece_width = expert_piece.shape[4]
    routed_total = jnp.einsum(
        "tsecf,efd->tsecd", expert_piece, w_down, preferred_element_type=jnp.float32
    )
    shared_total = jnp.dot(
        shared_piece.reshape(tok_dev, piece_width), shared_down, preferred_element_type=jnp.float32
    )
    returned = lax.all_to_all(
        routed_total.astype(jnp.bfloat16), "sp", split_axis=1, concat_axis=1, tiled=True
    )
    returned = returned.reshape(n_tp, slot_count, d_dev).astype(jnp.float32)
    routed = jnp.einsum("tmr,tmd->trd", combine_table, returned, precision=lax.Precision.HIGHEST)
    routed = routed.reshape(tok_dev, d_dev)
    return (residual + routed + shared_total).astype(jnp.bfloat16)


def solution(mesh):
    placed = (
        P("sp", "tp"),
        P("sp", None),
        P("sp", None),
        P("tp"),
        P("tp", None),
        P(("sp", "tp"), None),
        P(),
        P("sp", None),
        P("sp", None),
        P("sp", "tp", None),
        P("sp", "tp", None),
        P("sp", None, "tp"),
        P("tp", None),
        P("tp", None),
        P(None, "tp"),
    )
    return jax.shard_map(
        local, mesh=mesh, in_specs=placed, out_specs=P("sp", "tp"), check_vma=False
    )
```

profile of v0, /device:TPU:0, one launch (start us, length us, event | category | flops | bytes accessed | tf_op | source)
XLA Modules:
  0.0 317.8 jit_solution(6857469026317906916)
XLA Ops:
  6.5 1.1 constant_dynamic-slice_fusion
  7.7 4.9 %collective-permute-start = (bf16[128,128]{1,0:T(8,128)(2,1)S(1)}, bf16[128,128]{1,0:T(8,128)(2,1)S(1)}, u32[]{:S(2)}, u32[]{:S(2)}) collective-permute-start(bf16[128,128]{1,0:T(8,128)(2,1)S(1)} %get-tuple-element.10), channel_id=1, source_target_pairs={{0,4},{4,8},{8,12},{12,16},{16,20},{20,24},{24,28},{1,5},{5,9},{9,... | collective-permute-start | bytes 98312 | tf_op jit(solution)/shard_map/ppermute | solution.py:23
  12.6 1.3 collective-permute-start.1
  14.6 1.1 reshape.199
  15.7 2.7 collective-permute-done.1
  20.4 1.8 fusion.27
  22.3 32.5 %reduce-scatter.2.cloned.1.call-done = f32[64,2048]{1,0:T(8,128)} async-done(((f32[256,2048]{1,0:T(8,128)}), f32[64,2048]{1,0:T(8,128)}) %reduce-scatter.2.cloned.1.call-update) | async-done | bytes 524304 | tf_op jit(solution)/shard_map/reduce_scatter | solution.py:97
  54.7 1.8 add_convert_fusion
  57.2 2.4 reduce-window.6
  60.4 1.3 convert_reduce_fusion
  61.7 11.7 %all-gather.5.cloned.1.call-done = bf16[256,2048]{1,0:T(8,128)(2,1)} async-done(((bf16[64,2048]{1,0:T(8,128)(2,1)}), bf16[256,2048]{1,0:T(8,128)(2,1)}) %all-gather.5.cloned.1.call-update) | async-done | bytes 1048592 | tf_op jit(solution)/shard_map/all_gather | solution.py:104
  73.4 1.5 multiply_reduce_fusion
  74.9 1.5 multiply_convert_fusion
  76.5 0.7 convolution_convert_fusion
  77.2 53.9 %all_to_all.14 = bf16[8,64,2048]{2,1,0:T(8,128)(2,1)S(1)} all-to-all(bf16[8,64,2048]{2,1,0:T(8,128)(2,1)S(1)} %bitcast.114), channel_id=1, replica_groups=mesh['sp'=8,'tp'=4] {'sp'}, dimensions={0} | all-to-all | bytes 4194304 | tf_op jit(solution)/shard_map/all_to_all | solution.py:122
  131.1 1.5 copy.68
  132.8 56.3 %all-gather.7.cloned.1.call-done = bf16[4,8,8,8,2048]{4,3,1,0,2:T(8,128)(2,1)} async-done(((bf16[1,8,8,8,2048]{4,3,1,0,2:T(8,128)(2,1)}), bf16[4,8,8,8,2048]{4,3,1,0,2:T(8,128)(2,1)}) %all-gather.7.cloned.1.call-update) | async-done | bytes 8388624 | tf_op jit(solution)/shard_map/all_gather | solution.py:124
  189.2 8.1 %fusion.4 = f32[8,4,8,8,256]{4,3,2,1,0:T(8,128)S(1)} fusion(bf16[4,8,8,8,2048]{4,3,1,0,2:T(8,128)(2,1)} %all-gather.7.cloned.1.call-done, bf16[8,256,2048]{2,1,0:T(8,128)(2,1)} %param.24), kind=kOutput, calls=%fused_computation.4 | convolution fusion | flops 2147483648 | bytes 18874368 | tf_op jit(solution)/shard_map/tsecd,efd->tsecf/dot_general | solution.py:125
  197.3 11.4 %fusion.6 = bf16[4,8,8,8,256]{4,3,1,0,2:T(8,128)(2,1)} fusion(f32[8,4,8,8,256]{4,3,2,1,0:T(8,128)S(1)} %fusion.4, bf16[4,8,8,8,2048]{4,3,1,0,2:T(8,128)(2,1)} %all-gather.7.cloned.1.call-done, bf16[8,256,2048]{2,1,0:T(8,128)(2,1)} %param.25), kind=kOutput, calls=%fused_computation.8 | convolution fusion | flops 2150629376 | bytes 19922944 | tf_op jit(solution)/shard_map/tsecd,efd->tsecf/dot_general | solution.py:128
  208.7 35.2 %all-gather.9.cloned.1.call-done = bf16[4,8,8,8,1024]{4,3,1,0,2:T(8,128)(2,1)} async-done(((bf16[4,8,8,8,256]{4,3,1,0,2:T(8,128)(2,1)}), bf16[4,8,8,8,1024]{4,3,1,0,2:T(8,128)(2,1)}) %all-gather.9.cloned.1.call-update) | async-done | bytes 4194320 | tf_op jit(solution)/shard_map/all_gather | solution.py:136
  243.8 7.0 %convert_bitcast_fusion = bf16[4,8,8,8,512]{4,3,1,0,2:T(8,128)(2,1)S(1)} fusion(bf16[4,8,8,8,1024]{4,3,1,0,2:T(8,128)(2,1)} %all-gather.9.cloned.1.call-done, bf16[8,1024,512]{2,1,0:T(8,128)(2,1)} %param.26), kind=kOutput, calls=%fused_computation.14 | convolution fusion | flops 2148532224 | bytes 14680064 | tf_op jit(solution)/shard_map/tsecf,efd->tsecd/dot_general | solution.py:139
  250.8 1.6 copy.69
  252.4 5.6 %all-to-all-start.1 = ((bf16[4,8,8,8,512]{4,3,0,2,1:T(8,128)(2,1)}), bf16[4,8,8,8,512]{4,3,0,2,1:T(8,128)(2,1)S(1)}, u32[]{:S(2)}, u32[]{:S(2)}) async-start(bf16[4,8,8,8,512]{4,3,0,2,1:T(8,128)(2,1)} %copy.69), calls=%async_computation.2 | async-start | bytes 4194304 | tf_op jit(solution)/shard_map/all_to_all | solution.py:145
  258.1 1.6 convert_element_type.61
  259.7 0.7 copy-done.7
  260.8 0.5 fusion.16
  261.3 7.4 %all-gather = bf16[256,1024]{1,0:T(8,128)(2,1)} all-gather(bf16[256,256]{1,0:T(8,128)(2,1)S(1)} %fusion.16), channel_id=2, replica_groups=mesh['sp'=8,'tp'=4] {'tp'}, dimensions={1}, use_global_device_ids=true | all-gather | bytes 655360 | tf_op jit(solution)/shard_map/all_gather | solution.py:137
  268.7 38.0 %all-to-all-done.1 = bf16[4,8,8,8,512]{4,3,0,2,1:T(8,128)(2,1)S(1)} async-done(((bf16[4,8,8,8,512]{4,3,0,2,1:T(8,128)(2,1)}), bf16[4,8,8,8,512]{4,3,0,2,1:T(8,128)(2,1)S(1)}, u32[]{:S(2)}, u32[]{:S(2)}) %all-to-all-start.1) | async-done | bytes 2097184 | tf_op jit(solution)/shard_map/all_to_all | solution.py:145
  307.0 0.8 copy-done.6
  307.8 1.2 fusion.42
  308.9 1.1 bitcast_add_fusion
  310.1 1.1 fusion.15
  (76 shorter events, 5.2 us)
Async XLA Ops:
  6.5 13.8 %copy-start = (bf16[256,2048]{1,0:T(8,128)(2,1)S(1)}, bf16[256,2048]{1,0:T(8,128)(2,1)}, u32[]{:S(2)}) copy-start(bf16[256,2048]{1,0:T(8,128)(2,1)} %param.19) | copy-start | bytes 3145732
  6.5 48.2 %reduce-scatter.2.cloned.1.call-start = ((), (), s32[]{:S(2)}) async-start(), calls=%async_computation.3 | async-start | bytes 2621440 | tf_op jit(solution)/shard_map/reduce_scatter | solution.py:97
  6.5 12.9 %copy-start.13 = (f32[4]{0:T(128)S(1)}, f32[4]{0:T(128)}, u32[]{:S(2)}) copy-start(f32[4]{0:T(128)} %param.18) | copy-start | bytes 52
  7.7 8.0 %collective-permute-start = (bf16[128,128]{1,0:T(8,128)(2,1)S(1)}, bf16[128,128]{1,0:T(8,128)(2,1)S(1)}, u32[]{:S(2)}, u32[]{:S(2)}) collective-permute-start(bf16[128,128]{1,0:T(8,128)(2,1)S(1)} %get-tuple-element.10), channel_id=1, source_target_pairs={{0,4},{4,8},{8,12},{12,16},{16,20},{20,24},{24,28},{1,5},{5,9},{9,... | collective-permute-start | bytes 98312 | tf_op jit(solution)/shard_map/ppermute | solution.py:23
  12.6 5.8 %collective-permute-start.1 = (bf16[128,128]{1,0:T(8,128)(2,1)S(1)}, bf16[128,128]{1,0:T(8,128)(2,1)S(1)}, u32[]{:S(2)}, u32[]{:S(2)}) collective-permute-start(bf16[128,128]{1,0:T(8,128)(2,1)S(1)} %get-tuple-element.11), channel_id=1, source_target_pairs={{4,0},{8,4},{12,8},{16,12},{20,16},{24,20},{28,24},{5,1},{9,5},{13... | collective-permute-start | bytes 98312 | tf_op jit(solution)/shard_map/ppermute | solution.py:24
  20.4 34.4 %copy-start.9 = (bf16[64,2048]{1,0:T(8,128)(2,1)S(1)}, bf16[64,2048]{1,0:T(8,128)(2,1)}, u32[]{:S(2)}) copy-start(bf16[64,2048]{1,0:T(8,128)(2,1)} %param.20) | copy-start | bytes 786436
  22.2 34.4 %copy-start.10 = (s32[256,4]{0,1:T(4,128)S(1)}, s32[256,4]{0,1:T(4,128)}, u32[]{:S(2)}) copy-start(s32[256,4]{0,1:T(4,128)} %param.22) | copy-start | bytes 12292
  22.2 38.1 %copy-start.11 = (f32[256,4]{0,1:T(4,128)S(1)}, f32[256,4]{0,1:T(4,128)}, u32[]{:S(2)}) copy-start(f32[256,4]{0,1:T(4,128)} %param.23) | copy-start | bytes 12292
  22.2 38.2 %copy-start.12 = (bf16[2048]{0:T(1024)(128)(2,1)S(1)}, bf16[2048]{0:T(1024)(128)(2,1)}, u32[]{:S(2)}) copy-start(bf16[2048]{0:T(1024)(128)(2,1)} %param.21) | copy-start | bytes 12292
  22.2 51.2 %all-gather.5.cloned.1.call-start = ((), (), s32[]{:S(2)}) async-start(), calls=%async_computation.4 | async-start | bytes 1310720 | tf_op jit(solution)/shard_map/all_gather | solution.py:104
  56.5 132.6 %all-gather.7.cloned.1.call-start = ((), (), s32[]{:S(2)}) async-start(), calls=%async_computation.5 | async-start | bytes 10485760 | tf_op jit(solution)/shard_map/all_gather | solution.py:124
  76.5 54.6 %copy-start.3 = (bf16[256,2048]{1,0:T(8,128)(2,1)}, bf16[256,2048]{1,0:T(8,128)(2,1)S(1)}, u32[]{:S(2)}) copy-start(bf16[256,2048]{1,0:T(8,128)(2,1)S(1)} %multiply_convert_fusion) | copy-start | bytes 3145732
  132.6 111.2 %all-gather.9.cloned.1.call-start = ((), (), s32[]{:S(2)}) async-start(), calls=%async_computation.6 | async-start | bytes 5242880 | tf_op jit(solution)/shard_map/all_gather | solution.py:136
  252.4 5.6 %copy-start.2 = (bf16[256,2048]{1,0:T(8,128)(2,1)S(1)}, bf16[256,2048]{1,0:T(8,128)(2,1)}, u32[]{:S(2)}) copy-start(bf16[256,2048]{1,0:T(8,128)(2,1)} %all-gather.5.cloned.1.call-done) | copy-start | bytes 3145732
  252.4 54.3 %all-to-all-start.1 = ((bf16[4,8,8,8,512]{4,3,0,2,1:T(8,128)(2,1)}), bf16[4,8,8,8,512]{4,3,0,2,1:T(8,128)(2,1)S(1)}, u32[]{:S(2)}, u32[]{:S(2)}) async-start(bf16[4,8,8,8,512]{4,3,0,2,1:T(8,128)(2,1)} %copy.69), calls=%async_computation.2 | async-start | bytes 4194304 | tf_op jit(solution)/shard_map/all_to_all | solution.py:145
  258.1 1.6 copy-start.4
  258.1 2.3 copy-start.7
  258.1 2.8 copy-start.14
  306.7 1.0 copy-start.6
  307.8 2.3 copy-start.5
  307.8 2.3 copy-start.8
  307.8 3.5 %copy-start.1 = (bf16[256,2048]{1,0:T(8,128)(2,1)S(1)}, bf16[256,2048]{1,0:T(8,128)(2,1)}, u32[]{:S(2)}) copy-start(bf16[256,2048]{1,0:T(8,128)(2,1)} %param.19) | copy-start | bytes 3145732
Sparse Core Ops, SparseCore 0:
  22.3 32.3 reduce-scatter.1
  56.7 16.6 all-gather.4
  132.7 56.3 all-gather.6
  208.8 34.9 all-gather.8
where the time goes:
time: 318 us
  waiting for transfers between devices  176 us (55%)
  blocking collectives  61.2 us (19%)
  matrix products  33.1 us (10%)
  between operations  13.5 us (4%)
  other arithmetic  12.7 us (4%)
  starting transfers between devices  12.1 us (4%)
  local copies, waits for them, and re-layouts  8.65 us (3%)
    all_gather x1, waiting for transfers between devices, local(): piece_rows = lax.all_gather(arrived, 'tp', axis=0, tiled=True)  56.3 us
    all_to_all x1, blocking collectives, local(): lax.all_to_all(outgoing, 'sp', split_axis=0, concat_axis=0, tiled=True)  53.9 us
    all_to_all x1, waiting for transfers between devices, local(): lax.all_to_all(routed_total.astype(jnp.bfloat16), 'sp', split_axis=1, con...  38 us
    all_gather x1, waiting for transfers between devices, local(): expert_piece = lax.all_gather(hidden, 'tp', axis=4, tiled=True)  35.2 us
    reduce_scatter x1, waiting for transfers between devices, local(): lax.psum_scatter(jnp.dot(attended, w_out, preferred_element_type=jnp.floa...  32.5 us
    all_gather x1, waiting for transfers between devices, local(): whole_rows = lax.all_gather(mixed_rows, 'tp', axis=0, tiled=True)  11.7 us
    dot_general x1, matrix products, local(): jnp.einsum('tsecd,efd->tsecf', piece_rows, w_up, preferred_element_type=j...  11.4 us
    dot_general x1, matrix products, local(): jnp.einsum('tsecd,efd->tsecf', piece_rows, w_gate, preferred_element_type...  8.13 us
  transfers between devices with their start and end apart: 7, of which 6 were waited for; matrix products, arithmetic and copies ran while one was open for 3% of the time, Pallas kernels for 0%

commit v1 on v0

--- a/solution.py
+++ b/solution.py
@@ -1,3 +1,4 @@
+import functools
 import jax
 import jax.numpy as jnp
 from jax import lax
@@ -11,6 +12,17 @@
 EXPERTS = 64
 TOPK = 4
 NORM_EPS = 1e-05
+
+
+def spread_roads(xs, mesh_name):
+    piece_now = jax.lax.psum(1, mesh_name)
+    newest = jnp.split(xs, piece_now, axis=1)
+    z2 = jnp.stack(newest, axis=0)
+    d_next = jax.lax.all_to_all(z2, mesh_name, 0, 0)
+    return jnp.concatenate(d_next, 1)
+
+
+render_vectors = functools.partial(spread_roads, mesh_name="sp")
 
 
 def with_halo(array, sides, width):
@@ -142,9 +154,7 @@
     shared_total = jnp.dot(
         shared_piece.reshape(tok_dev, piece_width), shared_down, preferred_element_type=jnp.float32
     )
-    returned = lax.all_to_all(
-        routed_total.astype(jnp.bfloat16), "sp", split_axis=1, concat_axis=1, tiled=True
-    )
+    returned = render_vectors(routed_total.astype(jnp.bfloat16))
     returned = returned.reshape(n_tp, slot_count, d_dev).astype(jnp.float32)
     routed = jnp.einsum("tmr,tmd->trd", combine_table, returned, precision=lax.Precision.HIGHEST)
     routed = routed.reshape(tok_dev, d_dev)

time: 318 us -> 322 us (1.013)
  local copies, waits for them, and re-layouts: 8.65 us -> 12.8 us
    unnamed x31 -> x38, local copies, waits for them, and re-layouts: 1.66 us -> 6.71 us
where the time goes in v1:
time: 322 us
  waiting for transfers between devices  176 us (55%)
  blocking collectives  61.2 us (19%)
  matrix products  33.1 us (10%)
  between operations  13.5 us (4%)
  local copies, waits for them, and re-layouts  12.8 us (4%)
  other arithmetic  12.7 us (4%)
  starting transfers between devices  12.1 us (4%)
    all_gather x1, waiting for transfers between devices, local(): piece_rows = lax.all_gather(arrived, 'tp', axis=0, tiled=True)  56.3 us
    all_to_all x1, blocking collectives, local(): lax.all_to_all(outgoing, 'sp', split_axis=0, concat_axis=0, tiled=True)  53.9 us
    all_to_all x1, waiting for transfers between devices, spread_roads(): d_next = jax.lax.all_to_all(z2, mesh_name, 0, 0)  38 us
    all_gather x1, waiting for transfers between devices, local(): expert_piece = lax.all_gather(hidden, 'tp', axis=4, tiled=True)  35.2 us
    reduce_scatter x1, waiting for transfers between devices, local(): lax.psum_scatter(jnp.dot(attended, w_out, preferred_element_type=jnp.floa...  32.5 us
    all_gather x1, waiting for transfers between devices, local(): whole_rows = lax.all_gather(mixed_rows, 'tp', axis=0, tiled=True)  11.7 us
    dot_general x1, matrix products, local(): jnp.einsum('tsecd,efd->tsecf', piece_rows, w_up, preferred_element_type=j...  11.4 us
    dot_general x1, matrix products, local(): jnp.einsum('tsecd,efd->tsecf', piece_rows, w_gate, preferred_element_type...  8.13 us
  transfers between devices with their start and end apart: 7, of which 6 were waited for; matrix products, arithmetic and copies ran while one was open for 3% of the time, Pallas kernels for 0%

profile of v1, /device:TPU:0, one launch (start us, length us, event | category | flops | bytes accessed | tf_op | source)
XLA Modules:
  0.0 322.0 jit_solution(17035566820541005674)
XLA Ops:
  6.5 1.1 constant_dynamic-slice_fusion
  7.7 4.9 %collective-permute-start = (bf16[128,128]{1,0:T(8,128)(2,1)S(1)}, bf16[128,128]{1,0:T(8,128)(2,1)S(1)}, u32[]{:S(2)}, u32[]{:S(2)}) collective-permute-start(bf16[128,128]{1,0:T(8,128)(2,1)S(1)} %get-tuple-element.10), channel_id=1, source_target_pairs={{0,4},{4,8},{8,12},{12,16},{16,20},{20,24},{24,28},{1,5},{5,9},{9,... | collective-permute-start | bytes 98312 | tf_op jit(solution)/shard_map/ppermute | solution.py:35
  12.6 1.3 collective-permute-start.1
  14.6 1.1 reshape.199
  15.7 2.7 collective-permute-done.1
  20.4 1.8 fusion.35
  22.3 32.5 %reduce-scatter.2.cloned.1.call-done = f32[64,2048]{1,0:T(8,128)} async-done(((f32[256,2048]{1,0:T(8,128)}), f32[64,2048]{1,0:T(8,128)}) %reduce-scatter.2.cloned.1.call-update) | async-done | bytes 524304 | tf_op jit(solution)/shard_map/reduce_scatter | solution.py:109
  54.7 1.8 add_convert_fusion
  57.2 2.4 reduce-window.6
  60.4 1.3 convert_reduce_fusion
  61.7 11.7 %all-gather.5.cloned.1.call-done = bf16[256,2048]{1,0:T(8,128)(2,1)} async-done(((bf16[64,2048]{1,0:T(8,128)(2,1)}), bf16[256,2048]{1,0:T(8,128)(2,1)}) %all-gather.5.cloned.1.call-update) | async-done | bytes 1048592 | tf_op jit(solution)/shard_map/all_gather | solution.py:116
  73.4 1.5 multiply_reduce_fusion
  74.9 1.5 multiply_convert_fusion
  76.5 0.7 convolution_convert_fusion
  77.2 53.9 %all_to_all.14 = bf16[8,64,2048]{2,1,0:T(8,128)(2,1)S(1)} all-to-all(bf16[8,64,2048]{2,1,0:T(8,128)(2,1)S(1)} %bitcast.162), channel_id=1, replica_groups=mesh['sp'=8,'tp'=4] {'sp'}, dimensions={0} | all-to-all | bytes 4194304 | tf_op jit(solution)/shard_map/all_to_all | solution.py:134
  131.1 1.5 copy.65
  132.8 56.3 %all-gather.7.cloned.1.call-done = bf16[4,8,8,8,2048]{4,3,1,0,2:T(8,128)(2,1)} async-done(((bf16[1,8,8,8,2048]{4,3,1,0,2:T(8,128)(2,1)}), bf16[4,8,8,8,2048]{4,3,1,0,2:T(8,128)(2,1)}) %all-gather.7.cloned.1.call-update) | async-done | bytes 8388624 | tf_op jit(solution)/shard_map/all_gather | solution.py:136
  189.2 8.1 %fusion.4 = f32[8,4,8,8,256]{4,3,2,1,0:T(8,128)S(1)} fusion(bf16[4,8,8,8,2048]{4,3,1,0,2:T(8,128)(2,1)} %all-gather.7.cloned.1.call-done, bf16[8,256,2048]{2,1,0:T(8,128)(2,1)} %param.24), kind=kOutput, calls=%fused_computation.4 | convolution fusion | flops 2147483648 | bytes 18874368 | tf_op jit(solution)/shard_map/tsecd,efd->tsecf/dot_general | solution.py:137
  197.3 11.4 %fusion.6 = bf16[4,8,8,8,256]{4,3,1,0,2:T(8,128)(2,1)} fusion(f32[8,4,8,8,256]{4,3,2,1,0:T(8,128)S(1)} %fusion.4, bf16[4,8,8,8,2048]{4,3,1,0,2:T(8,128)(2,1)} %all-gather.7.cloned.1.call-done, bf16[8,256,2048]{2,1,0:T(8,128)(2,1)} %param.25), kind=kOutput, calls=%fused_computation.8 | convolution fusion | flops 2150629376 | bytes 19922944 | tf_op jit(solution)/shard_map/tsecd,efd->tsecf/dot_general | solution.py:140
  208.7 35.2 %all-gather.9.cloned.1.call-done = bf16[4,8,8,8,1024]{4,3,1,0,2:T(8,128)(2,1)} async-done(((bf16[4,8,8,8,256]{4,3,1,0,2:T(8,128)(2,1)}), bf16[4,8,8,8,1024]{4,3,1,0,2:T(8,128)(2,1)}) %all-gather.9.cloned.1.call-update) | async-done | bytes 4194320 | tf_op jit(solution)/shard_map/all_gather | solution.py:148
  243.8 7.0 %convert_bitcast_fusion = bf16[4,8,8,8,512]{4,3,1,0,2:T(8,128)(2,1)S(1)} fusion(bf16[4,8,8,8,1024]{4,3,1,0,2:T(8,128)(2,1)} %all-gather.9.cloned.1.call-done, bf16[8,1024,512]{2,1,0:T(8,128)(2,1)} %param.26), kind=kOutput, calls=%fused_computation.14 | convolution fusion | flops 2148532224 | bytes 14680064 | tf_op jit(solution)/shard_map/tsecf,efd->tsecd/dot_general | solution.py:151
  251.5 0.7 fusion.29
  253.0 0.7 fusion.27
  255.2 0.7 fusion.24
  256.6 5.6 %all-to-all-start.1 = ((bf16[8,4,1,8,8,512]{5,4,1,3,2,0:T(8,128)(2,1)}), bf16[8,4,1,8,8,512]{5,4,1,3,2,0:T(8,128)(2,1)S(1)}, u32[]{:S(2)}, u32[]{:S(2)}) async-start(bf16[8,4,1,8,8,512]{5,4,1,3,2,0:T(8,128)(2,1)} %fusion.23), calls=%async_computation.2 | async-start | bytes 4194304 | tf_op jit(solution)/shard_map/all_to_all | solution.py:21
  262.3 1.6 convert_element_type.61
  265.5 7.4 %all-gather = bf16[256,1024]{1,0:T(8,128)(2,1)} all-gather(bf16[256,256]{1,0:T(8,128)(2,1)S(1)} %fusion.16), channel_id=2, replica_groups=mesh['sp'=8,'tp'=4] {'tp'}, dimensions={1}, use_global_device_ids=true | all-gather | bytes 655360 | tf_op jit(solution)/shard_map/all_gather | solution.py:149
  272.9 38.0 %all-to-all-done.1 = bf16[8,4,1,8,8,512]{5,4,1,3,2,0:T(8,128)(2,1)S(1)} async-done(((bf16[8,4,1,8,8,512]{5,4,1,3,2,0:T(8,128)(2,1)}), bf16[8,4,1,8,8,512]{5,4,1,3,2,0:T(8,128)(2,1)S(1)}, u32[]{:S(2)}, u32[]{:S(2)}) %all-to-all-start.1) | async-done | bytes 2097184 | tf_op jit(solution)/shard_map/all_to_all | solution.py:21
  311.2 0.8 copy-done.6
  311.9 1.2 fusion.50
  313.1 1.1 bitcast_add_fusion
  314.3 1.1 fusion.15
  (83 shorter events, 9.9 us)
Async XLA Ops:
  6.5 13.8 %copy-start = (bf16[256,2048]{1,0:T(8,128)(2,1)S(1)}, bf16[256,2048]{1,0:T(8,128)(2,1)}, u32[]{:S(2)}) copy-start(bf16[256,2048]{1,0:T(8,128)(2,1)} %param.19) | copy-start | bytes 3145732
  6.5 48.2 %reduce-scatter.2.cloned.1.call-start = ((), (), s32[]{:S(2)}) async-start(), calls=%async_computation.3 | async-start | bytes 2621440 | tf_op jit(solution)/shard_map/reduce_scatter | solution.py:109
  6.5 12.9 %copy-start.13 = (f32[4]{0:T(128)S(1)}, f32[4]{0:T(128)}, u32[]{:S(2)}) copy-start(f32[4]{0:T(128)} %param.18) | copy-start | bytes 52
  7.7 8.0 %collective-permute-start = (bf16[128,128]{1,0:T(8,128)(2,1)S(1)}, bf16[128,128]{1,0:T(8,128)(2,1)S(1)}, u32[]{:S(2)}, u32[]{:S(2)}) collective-permute-start(bf16[128,128]{1,0:T(8,128)(2,1)S(1)} %get-tuple-element.10), channel_id=1, source_target_pairs={{0,4},{4,8},{8,12},{12,16},{16,20},{20,24},{24,28},{1,5},{5,9},{9,... | collective-permute-start | bytes 98312 | tf_op jit(solution)/shard_map/ppermute | solution.py:35
  12.6 5.8 %collective-permute-start.1 = (bf16[128,128]{1,0:T(8,128)(2,1)S(1)}, bf16[128,128]{1,0:T(8,128)(2,1)S(1)}, u32[]{:S(2)}, u32[]{:S(2)}) collective-permute-start(bf16[128,128]{1,0:T(8,128)(2,1)S(1)} %get-tuple-element.11), channel_id=1, source_target_pairs={{4,0},{8,4},{12,8},{16,12},{20,16},{24,20},{28,24},{5,1},{9,5},{13... | collective-permute-start | bytes 98312 | tf_op jit(solution)/shard_map/ppermute | solution.py:36
  20.4 34.4 %copy-start.9 = (bf16[64,2048]{1,0:T(8,128)(2,1)S(1)}, bf16[64,2048]{1,0:T(8,128)(2,1)}, u32[]{:S(2)}) copy-start(bf16[64,2048]{1,0:T(8,128)(2,1)} %param.20) | copy-start | bytes 786436
  22.2 34.4 %copy-start.10 = (s32[256,4]{0,1:T(4,128)S(1)}, s32[256,4]{0,1:T(4,128)}, u32[]{:S(2)}) copy-start(s32[256,4]{0,1:T(4,128)} %param.22) | copy-start | bytes 12292
  22.2 38.1 %copy-start.11 = (f32[256,4]{0,1:T(4,128)S(1)}, f32[256,4]{0,1:T(4,128)}, u32[]{:S(2)}) copy-start(f32[256,4]{0,1:T(4,128)} %param.23) | copy-start | bytes 12292
  22.2 38.2 %copy-start.12 = (bf16[2048]{0:T(1024)(128)(2,1)S(1)}, bf16[2048]{0:T(1024)(128)(2,1)}, u32[]{:S(2)}) copy-start(bf16[2048]{0:T(1024)(128)(2,1)} %param.21) | copy-start | bytes 12292
  22.2 51.2 %all-gather.5.cloned.1.call-start = ((), (), s32[]{:S(2)}) async-start(), calls=%async_computation.4 | async-start | bytes 1310720 | tf_op jit(solution)/shard_map/all_gather | solution.py:116
  56.5 132.6 %all-gather.7.cloned.1.call-start = ((), (), s32[]{:S(2)}) async-start(), calls=%async_computation.5 | async-start | bytes 10485760 | tf_op jit(solution)/shard_map/all_gather | solution.py:136
  76.5 54.6 %copy-start.3 = (bf16[256,2048]{1,0:T(8,128)(2,1)}, bf16[256,2048]{1,0:T(8,128)(2,1)S(1)}, u32[]{:S(2)}) copy-start(bf16[256,2048]{1,0:T(8,128)(2,1)S(1)} %multiply_convert_fusion) | copy-start | bytes 3145732
  132.6 111.2 %all-gather.9.cloned.1.call-start = ((), (), s32[]{:S(2)}) async-start(), calls=%async_computation.6 | async-start | bytes 5242880 | tf_op jit(solution)/shard_map/all_gather | solution.py:148
  256.6 5.6 %copy-start.2 = (bf16[256,2048]{1,0:T(8,128)(2,1)S(1)}, bf16[256,2048]{1,0:T(8,128)(2,1)}, u32[]{:S(2)}) copy-start(bf16[256,2048]{1,0:T(8,128)(2,1)} %all-gather.5.cloned.1.call-done) | copy-start | bytes 3145732
  256.6 54.3 %all-to-all-start.1 = ((bf16[8,4,1,8,8,512]{5,4,1,3,2,0:T(8,128)(2,1)}), bf16[8,4,1,8,8,512]{5,4,1,3,2,0:T(8,128)(2,1)S(1)}, u32[]{:S(2)}, u32[]{:S(2)}) async-start(bf16[8,4,1,8,8,512]{5,4,1,3,2,0:T(8,128)(2,1)} %fusion.23), calls=%async_computation.2 | async-start | bytes 4194304 | tf_op jit(solution)/shard_map/all_to_all | solution.py:21
  262.3 1.6 copy-start.4
  262.3 2.3 copy-start.7
  262.3 2.8 copy-start.14
  310.9 1.0 copy-start.6
  311.9 2.3 copy-start.5
  311.9 2.3 copy-start.8
  311.9 3.5 %copy-start.1 = (bf16[256,2048]{1,0:T(8,128)(2,1)S(1)}, bf16[256,2048]{1,0:T(8,128)(2,1)}, u32[]{:S(2)}) copy-start(bf16[256,2048]{1,0:T(8,128)(2,1)} %param.19) | copy-start | bytes 3145732
Sparse Core Ops, SparseCore 0:
  22.3 32.3 reduce-scatter.1
  56.7 16.6 all-gather.4
  132.7 56.3 all-gather.6
  208.8 34.9 all-gather.8
